TPU v7x, 512 devices: a 4x2x32 block of a 4x8x32 slice. The times are simulated.
512 devices in a mesh: grp: 2 (over y), fs: 32 (over z), tp: 8 (over x, core).
Axes of the slice: x: 4, y: 2, z: 32, core: 2. Of those that a mesh axis runs over, the one named last changes fastest.
The devices are a block of a 4x8x32 slice.
Arguments:
- layer_input_tokens: bfloat16 [32768, 2048], P(('grp', 'fs')), parts along dimension 0, may hold values from -6 to 6
- attention_norm_gain: float32 [2048], replicated, may hold values from 0.1 to 1.9
- query_projection: bfloat16 [2048, 1024], P('fs', 'tp'), may hold values from -0.125 to 0.125
- key_projection: bfloat16 [2048, 1024], P('fs', 'tp'), may hold values from -0.125 to 0.125
- value_projection: bfloat16 [2048, 2048], P('fs', 'tp'), may hold values from -0.125 to 0.125
- decay_first_factor: bfloat16 [2048, 16], replicated, may hold values from -0.125 to 0.125
- decay_second_factor: bfloat16 [16, 1024], P(None, 'tp'), may hold values from -1.5 to 1.5
- decay_logit_bias: float32 [1024], P('tp'), may hold values from -0.5 to 6
- extra_log_decay: float32 [32768, 8], P(('grp', 'fs'), 'tp'), parts along dimension 0, may hold values from -0.7 to 0
- head_output_gain: float32 [256], replicated, may hold values from 0.1 to 1.9
- attention_output_projection: bfloat16 [2048, 2048], P(('tp', 'fs')), may hold values from -0.125 to 0.125
- feedforward_norm_gain: float32 [2048], replicated, may hold values from 0.1 to 1.9
- gate_projection: bfloat16 [2048, 5632], P('fs', 'tp'), may hold values from -0.125 to 0.125
- up_projection: bfloat16 [2048, 5632], P('fs', 'tp'), may hold values from -0.125 to 0.125
- down_projection: bfloat16 [5632, 2048], P(('tp', 'fs')), may hold values from -0.078125 to 0.078125
Outputs:
- result: bfloat16 [32768, 2048], P(('grp', 'fs')), parts along dimension 0
There are 2 independent parts, one for each index of `grp`. A program takes and returns all parts, laid end to end along the dimension named above; an argument that names none is the same for every part. Nothing has to cross between parts.
All inputs are finite; a program needn't handle non-finite values.
Results may differ from a plain program's by a relative error of at most 0.02.
Values may be sent and summed in bfloat16 or wider, within the bound.
A program may use at most 64 MiB of HBM per device.

v0:
```python
import jax
import jax.numpy as jnp
from jax import lax
from jax.sharding import PartitionSpec as P

BLOCK = 64


normed_gate = 16.0


def sent_together(arrays, axis, dim, along):
    widths = [a.shape[along] for a in arrays]
    both = jnp.concatenate(arrays, axis=along)
    whole = lax.all_gather(both, axis, axis=dim, tiled=True)
    return tuple(jnp.split(whole, [sum(widths[:k]) for k in range(1, len(widths))], axis=along))


def laid_out(tiles, dim):
    tiles = jnp.moveaxis(tiles, 0, dim)
    shape = tiles.shape
    return tiles.reshape(*shape[:dim], shape[dim] * shape[dim + 1], *shape[dim + 2 :])


def sent_to_all(value, axis):
    copies = jnp.broadcast_to(value, (lax.axis_size(axis), *value.shape))
    return lax.all_to_all(copies, axis, split_axis=0, concat_axis=0, tiled=True)


def gathered_copies(value, axis, dim):
    return laid_out(sent_to_all(value, axis), dim)


def in_blocks(value, dim, devices):
    shape = value.shape
    tiles = value.reshape(*shape[:dim], devices, shape[dim] // devices, *shape[dim + 1 :])
    return jnp.moveaxis(tiles, dim, 0)


def sent_and_summed(value, axis, dim):
    tiles = in_blocks(value, dim, lax.axis_size(axis))
    arrived = lax.all_to_all(tiles, axis, split_axis=0, concat_axis=0, tiled=True)
    return arrived.astype(jnp.float32).sum(axis=0)


def norm_rows(values, gain):
    wide = values.astype(jnp.float32)
    scale = lax.rsqrt(jnp.mean(wide * wide, axis=-1, keepdims=True) + 1e-06)
    return wide * scale * gain


def block_scan(queries, keys, values, decays):
    length, key_channel_width = queries.shape
    value_width = values.shape[1]
    count = length // BLOCK
    lower_mask = jnp.arange(BLOCK)[:, None] >= jnp.arange(BLOCK)[None, :]

    def advance(carry, items):
        query_block, key_block, value_block, decay_block = items
        running = jnp.cumsum(decay_block, axis=0)
        middle = running[BLOCK // 2 - 1]
        closing = running[BLOCK - 1]
        carried = jnp.dot(query_block * jnp.exp(running), carry)
        scores = jnp.dot(
            query_block * jnp.exp(running - middle), (key_block * jnp.exp(middle - running)).T
        )
        scores = jnp.where(lower_mask, scores, 0.0)
        inside = jnp.dot(scores, value_block)
        fresh = carry * jnp.exp(closing)[:, None] + jnp.dot(
            (key_block * jnp.exp(closing - running)).T, value_block
        )
        return (fresh, carried + inside)

    items = (
        queries.reshape(count, BLOCK, key_channel_width),
        keys.reshape(count, BLOCK, key_channel_width),
        values.reshape(count, BLOCK, value_width),
        decays.reshape(count, BLOCK, key_channel_width),
    )
    _, outputs = lax.scan(advance, jnp.zeros((key_channel_width, value_width), jnp.float32), items)
    return outputs.reshape(length, value_width)


def both_ways(queries, keys, values, decays):
    ahead = block_scan(queries, keys, values, decays)
    behind = block_scan(
        jnp.flip(queries, 0), jnp.flip(keys, 0), jnp.flip(values, 0), jnp.flip(decays, 0)
    )
    return ahead + jnp.flip(behind, 0)


def head_norm(mixed, gain):
    scale = lax.rsqrt(jnp.mean(mixed * mixed, axis=-1, keepdims=True) + 1e-06)
    return mixed * scale * gain


def shards(
    layer_input_tokens,
    attention_norm_gain,
    query_projection,
    key_projection,
    value_projection,
    decay_first_factor,
    decay_second_factor,
    decay_logit_bias,
    extra_log_decay,
    head_output_gain,
    attention_output_projection,
    feedforward_norm_gain,
    gate_projection,
    up_projection,
    down_projection,
):
    rows = layer_input_tokens.shape[0]
    normed = norm_rows(layer_input_tokens, attention_norm_gain).astype(jnp.bfloat16)
    pieces = sent_together((query_projection, key_projection, value_projection), "fs", 0, 1)
    query, key, value = tuple(
        (jnp.dot(normed, piece, preferred_element_type=jnp.float32) for piece in pieces)
    )
    query = query.astype(jnp.bfloat16)
    key = key.astype(jnp.bfloat16)
    value = value.astype(jnp.bfloat16)
    lowrank = jnp.dot(normed, decay_first_factor, preferred_element_type=jnp.float32).astype(
        jnp.bfloat16
    )
    decay_logit_values = (
        jnp.dot(lowrank, decay_second_factor, preferred_element_type=jnp.float32) + decay_logit_bias
    )
    local_heads = extra_log_decay.shape[1]
    key_channel_width = query.shape[1] // local_heads
    value_width = value.shape[1] // local_heads
    decay_logarithm = jax.nn.log_sigmoid(decay_logit_values) / normed_gate + jnp.repeat(
        extra_log_decay, key_channel_width, axis=1
    )
    mixed = jax.vmap(both_ways, in_axes=1, out_axes=1)(
        query.astype(jnp.float32).reshape(rows, local_heads, key_channel_width),
        key.astype(jnp.float32).reshape(rows, local_heads, key_channel_width),
        value.astype(jnp.float32).reshape(rows, local_heads, value_width),
        decay_logarithm.reshape(rows, local_heads, key_channel_width),
    )
    headed = (
        head_norm(mixed, head_output_gain)
        .reshape(rows, local_heads * value_width)
        .astype(jnp.bfloat16)
    )
    share = rows // lax.axis_size("tp")
    out_full = gathered_copies(attention_output_projection, "fs", 0)
    mixer = sent_and_summed(
        jnp.dot(headed, out_full, preferred_element_type=jnp.float32).astype(jnp.bfloat16), "tp", 0
    )
    own = lax.dynamic_slice_in_dim(layer_input_tokens, lax.axis_index("tp") * share, share, 0)
    residual = (own.astype(jnp.float32) + mixer).astype(jnp.bfloat16)
    second = gathered_copies(
        norm_rows(residual, feedforward_norm_gain).astype(jnp.bfloat16), "tp", 0
    )
    gate_full, up_full = sent_together((gate_projection, up_projection), "fs", 0, 1)
    gate = jnp.dot(second, gate_full, preferred_element_type=jnp.float32)
    up = jnp.dot(second, up_full, preferred_element_type=jnp.float32)
    hidden = (jax.nn.silu(gate) * up).astype(jnp.bfloat16)
    down_full = lax.all_gather(down_projection, "fs", axis=0, tiled=True)
    channel = sent_and_summed(
        jnp.dot(hidden, down_full, preferred_element_type=jnp.float32).astype(jnp.bfloat16), "tp", 0
    )
    finished = (residual.astype(jnp.float32) + channel).astype(jnp.bfloat16)
    return gathered_copies(finished, "tp", 0)


def solution(mesh):
    placed = (
        P(("grp", "fs"), None),
        P(),
        P("fs", "tp"),
        P("fs", "tp"),
        P("fs", "tp"),
        P(),
        P(None, "tp"),
        P("tp"),
        P(("grp", "fs"), "tp"),
        P(),
        P(("tp", "fs"), None),
        P(),
        P("fs", "tp"),
        P("fs", "tp"),
        P(("tp", "fs"), None),
    )
    return jax.shard_map(
        shards, mesh=mesh, in_specs=placed, out_specs=P(("grp", "fs"), None), check_vma=False
    )
```

profile of v0, /device:TPU:33, one launch (start us, length us, event | category | flops | bytes accessed | tf_op | source)
XLA Modules:
  0.0 577.5 jit_solution(10488612066547851786)
XLA Ops:
  6.6 1.6 pad_maximum_fusion.1
  9.0 1.9 broadcast_in_dim.40
  10.9 46.4 %all-to-all-start = ((bf16[32,8,2048]{2,1,0:T(8,128)(2,1)}), bf16[32,8,2048]{2,1,0:T(8,128)(2,1)}, u32[]{:S(2)}, u32[]{:S(2)}) async-start(bf16[32,8,2048]{2,1,0:T(8,128)(2,1)} %broadcast_in_dim.40), calls=%async_computation | async-start | bytes 2097152 | tf_op jit(solution)/shard_map/all_to_all | solution.py:27
  58.9 1.9 fusion.102
  60.8 2.6 fusion.134
  64.8 146.1 %all-gather.5.cloned.1.call-done = bf16[2048,512]{1,0:T(8,128)(2,1)} async-done(((bf16[64,512]{1,0:T(8,128)(2,1)}), bf16[2048,512]{1,0:T(8,128)(2,1)}) %all-gather.5.cloned.1.call-update) | async-done | bytes 2097168 | tf_op jit(solution)/shard_map/all_gather | solution.py:15
  210.9 2.4 fusion.116
  214.6 2.6 fusion.113
  217.2 2.6 reverse.14
  219.9 2.4 fusion.115
  223.7 31.0 %while.27 = (s32[]{:T(128)}, f32[1,128,256]{2,1,0:T(8,128)S(1)}, f32[8,1,64,256]{3,2,1,0:T(8,128)S(1)}, f32[8,1,64,128]{3,2,1,0:T(8,128)}, f32[8,1,64,128]{3,2,1...) while((s32[]{:T(128)}, f32[1,128,256]{2,1,0:T(8,128)S(1)}, ...), condition=%wide.region_6.7_spmd.clone, body=%wide.region_4.6_spmd.clone.sunk | while | flops 12263427 | bytes 1057411 | solution.py:80
  255.0 31.0 %while.26 = (s32[]{:T(128)}, f32[1,128,256]{2,1,0:T(8,128)S(1)}, f32[8,1,64,256]{3,2,1,0:T(8,128)S(1)}, f32[8,1,64,128]{3,2,1,0:T(8,128)}, f32[8,1,64,128]{3,2,1...) while((s32[]{:T(128)}, f32[1,128,256]{2,1,0:T(8,128)S(1)}, ...), condition=%wide.region_3.4_spmd.clone, body=%wide.region_1.3_spmd.clone.sunk | while | flops 12263427 | bytes 1057411 | solution.py:80
  286.2 3.3 convolution_convert_fusion
  289.5 17.6 %all-to-all-start.1 = ((bf16[8,64,2048]{2,1,0:T(8,128)(2,1)}), bf16[8,64,2048]{2,1,0:T(8,128)(2,1)}, u32[]{:S(2)}, u32[]{:S(2)}) async-start(bf16[8,64,2048]{2,1,0:T(8,128)(2,1)} %bitcast.262), calls=%async_computation.1 | async-start | bytes 4194304 | tf_op jit(solution)/shard_map/all_to_all | solution.py:42
  307.1 26.3 %all-to-all-done.1 = bf16[8,64,2048]{2,1,0:T(8,128)(2,1)} async-done(((bf16[8,64,2048]{2,1,0:T(8,128)(2,1)}), bf16[8,64,2048]{2,1,0:T(8,128)(2,1)}, u32[]{:S(2)}, u32[]{:S(2)}) %all-to-all-start.1) | async-done | bytes 2097184 | tf_op jit(solution)/shard_map/all_to_all | solution.py:42
  333.4 2.0 convert_reduce_fusion.1
  335.8 1.6 broadcast_in_dim.41
  337.3 4.5 all-to-all-start.2
  341.8 4.5 reshape.591
  346.3 127.6 %all-gather.7.cloned.1.call-done = bf16[2048,1408]{1,0:T(8,128)(2,1)} async-done(((bf16[64,1408]{1,0:T(8,128)(2,1)}), bf16[2048,1408]{1,0:T(8,128)(2,1)}) %all-gather.7.cloned.1.call-update) | async-done | bytes 5767184 | tf_op jit(solution)/shard_map/all_gather | solution.py:15
  473.9 4.7 fusion.105
  478.6 9.1 %convolution_convert_fusion.1 = bf16[512,2048]{1,0:T(8,128)(2,1)} fusion(bf16[704,2048]{1,0:T(8,128)(2,1)} %reshape.591, bf16[512,2048]{1,0:T(8,128)(2,1)S(1)} %bitcast.267, bf16[2048,1408]{1,0:T(8,128)(2,1)} %all-gather.7.cloned.1.call-done, f32[512,704]{0,1:T(8,128)} %fusion.105), kind=kOutput, calls=%fused_computation.108 | convolution fusion | flops 2956001280 | bytes 11665408 | tf_op jit(solution)/shard_map/dot_general | solution.py:162
  487.7 51.5 %all_to_all.25 = bf16[8,64,2048]{2,1,0:T(8,128)(2,1)S(1)} all-to-all(bf16[8,64,2048]{2,1,0:T(8,128)(2,1)} %bitcast.268), channel_id=1, replica_groups=mesh['grp'=2,'fs'=32,'tp'=8] {'tp'}, dimensions={0} | all-to-all | bytes 4194304 | tf_op jit(solution)/shard_map/all_to_all | solution.py:42
  539.9 29.7 %all_to_all.26 = bf16[8,64,2048]{2,1,0:T(8,128)(2,1)S(1)} all-to-all(bf16[8,64,2048]{2,1,0:T(8,128)(2,1)S(1)} %broadcast_in_dim.42), channel_id=1, replica_groups=mesh['grp'=2,'fs'=32,'tp'=8] {'tp'}, dimensions={0} | all-to-all | bytes 4194304 | tf_op jit(solution)/shard_map/all_to_all | solution.py:27
  (169 shorter events, 70.5 us)
Async XLA Ops:
  6.5 54.2 %copy-start = (bf16[2048,16]{0,1:T(8,128)(2,1)S(1)}, bf16[2048,16]{0,1:T(8,128)(2,1)}, u32[]{:S(2)}) copy-start(bf16[2048,16]{0,1:T(8,128)(2,1)} %param.24) | copy-start | bytes 196612
  6.6 50.9 %copy-start.6 = (bf16[64,704]{1,0:T(8,128)(2,1)S(1)}, bf16[64,704]{1,0:T(8,128)(2,1)}, u32[]{:S(2)}) copy-start(bf16[64,704]{1,0:T(8,128)(2,1)} %param.32) | copy-start | bytes 270340
  6.6 50.9 %copy-start.7 = (bf16[64,704]{1,0:T(8,128)(2,1)S(1)}, bf16[64,704]{1,0:T(8,128)(2,1)}, u32[]{:S(2)}) copy-start(bf16[64,704]{1,0:T(8,128)(2,1)} %param.31) | copy-start | bytes 270340
  6.6 51.8 %copy-start.1 = (bf16[512,2048]{1,0:T(8,128)(2,1)S(1)}, bf16[512,2048]{1,0:T(8,128)(2,1)}, u32[]{:S(2)}) copy-start(bf16[512,2048]{1,0:T(8,128)(2,1)} %param.19) | copy-start | bytes 6291460
  6.6 204.3 %all-gather.5.cloned.1.call-start = ((), (), s32[]{:S(2)}) async-start(), calls=%async_computation.5 | async-start | bytes 2162688 | tf_op jit(solution)/shard_map/all_gather | solution.py:15
  8.2 333.6 %all-gather.9.cloned.1.call-start = ((), (), s32[]{:S(2)}) async-start(), calls=%async_computation.7 | async-start | bytes 3244032 | tf_op jit(solution)/shard_map/all_gather | solution.py:160
  10.9 47.9 %copy-start.8 = (f32[2048]{0:T(1024)S(1)}, f32[2048]{0:T(1024)}, u32[]{:S(2)}) copy-start(f32[2048]{0:T(1024)} %param.20) | copy-start | bytes 24580
  10.9 275.2 %all-to-all-start = ((bf16[32,8,2048]{2,1,0:T(8,128)(2,1)}), bf16[32,8,2048]{2,1,0:T(8,128)(2,1)}, u32[]{:S(2)}, u32[]{:S(2)}) async-start(bf16[32,8,2048]{2,1,0:T(8,128)(2,1)} %broadcast_in_dim.40), calls=%async_computation | async-start | bytes 2097152 | tf_op jit(solution)/shard_map/all_to_all | solution.py:27
  57.4 416.5 %all-gather.7.cloned.1.call-start = ((), (), s32[]{:S(2)}) async-start(), calls=%async_computation.6 | async-start | bytes 5947392 | tf_op jit(solution)/shard_map/all_gather | solution.py:15
  58.9 1.9 copy-start.11
  58.9 1.9 copy-start.12
  58.9 1.9 copy-start.13
  63.4 1.4 copy-start.5
  213.2 4.0 copy-start.2
  217.2 6.4 %copy-start.3 = (bf16[512,256]{1,0:T(8,128)(2,1)}, bf16[512,256]{1,0:T(8,128)(2,1)S(1)}, u32[]{:S(2)}) copy-start(bf16[512,256]{1,0:T(8,128)(2,1)S(1)} %fusion.113) | copy-start | bytes 786436
  222.2 1.4 copy-start.4
  255.0 31.2 %copy-start.10 = (f32[256]{0:T(256)S(1)}, f32[256]{0:T(256)}, u32[]{:S(2)}) copy-start(f32[256]{0:T(256)} %param.28) | copy-start | bytes 3076
  289.5 43.9 %all-to-all-start.1 = ((bf16[8,64,2048]{2,1,0:T(8,128)(2,1)}), bf16[8,64,2048]{2,1,0:T(8,128)(2,1)}, u32[]{:S(2)}, u32[]{:S(2)}) async-start(bf16[8,64,2048]{2,1,0:T(8,128)(2,1)} %bitcast.262), calls=%async_computation.1 | async-start | bytes 4194304 | tf_op jit(solution)/shard_map/all_to_all | solution.py:42
  307.1 28.6 %copy-start.9 = (f32[2048]{0:T(1024)S(1)}, f32[2048]{0:T(1024)}, u32[]{:S(2)}) copy-start(f32[2048]{0:T(1024)} %param.30) | copy-start | bytes 24580
  337.3 136.6 %all-to-all-start.2 = ((bf16[8,64,2048]{2,1,0:T(8,128)(2,1)}), bf16[8,64,2048]{2,1,0:T(8,128)(2,1)S(1)}, u32[]{:S(2)}, u32[]{:S(2)}) async-start(bf16[8,64,2048]{2,1,0:T(8,128)(2,1)} %broadcast_in_dim.41), calls=%async_computation.2 | async-start | bytes 4194304 | tf_op jit(solution)/shard_map/all_to_all | solution.py:27
Sparse Core Ops, SparseCore 0:
  9.5 201.3 all-gather.4
  213.0 124.3 all-gather.8
  339.5 134.3 all-gather.6
where the time goes:
time: 583 us; the launch traced here: 578 us
  waiting for transfers between devices  301 us (52%)
  blocking collectives  81.3 us (14%)
  matrix products  74.3 us (13%)
  starting transfers between devices  68.7 us (12%)
  local copies, waits for them, and re-layouts  29.1 us (5%)
  between operations  13.4 us (2%)
  other arithmetic  9.12 us (2%)
    all_gather x2, waiting for transfers between devices, sent_together(): whole = lax.all_gather(both, axis, axis=dim, tiled=True)  274 us
    all_to_all x1, blocking collectives, sent_and_summed(): lax.all_to_all(tiles, axis, split_axis=0, concat_axis=0, tiled=True)  51.5 us
    all_to_all x2, starting transfers between devices, sent_to_all(): return lax.all_to_all(copies, axis, split_axis=0, concat_axis=0, tiled=True)  50.9 us
    all_to_all x1, blocking collectives, sent_to_all(): return lax.all_to_all(copies, axis, split_axis=0, concat_axis=0, tiled=True)  29.7 us
    all_to_all x1, waiting for transfers between devices, sent_and_summed(): lax.all_to_all(tiles, axis, split_axis=0, concat_axis=0, tiled=True)  26.3 us
    all_to_all x1, starting transfers between devices, sent_and_summed(): lax.all_to_all(tiles, axis, split_axis=0, concat_axis=0, tiled=True)  17.6 us
    dot_general x16, matrix products, advance(): inside = jnp.dot(scores, value_block)  17.1 us
    dot_general x16, matrix products, advance(): jnp.dot((key_block * jnp.exp(closing - running)).T, value_block)  16 us
  transfers between devices with their start and end apart: 6, of which 3 were waited for; matrix products, arithmetic and copies ran while one was open for 16% of the time, Pallas kernels for 0%

commit v1 on v0

v1 whole, which is shorter than its diff:
```python
import functools

import jax
import jax.numpy as jnp
from jax import lax
from jax.experimental import pallas as pl
from jax.experimental.pallas import tpu as pltpu
from jax.sharding import PartitionSpec as P

MESH = pl.DeviceIdType.MESH
BLOCK = 64
LANES = 128
GATE = 16.0
EPS = 1e-06
CHUNKS = 2
F32 = jnp.float32
BF16 = jnp.bfloat16


def mm(a, b):
    return lax.dot_general(a, b, (((1,), (0,)), ((), ())), preferred_element_type=F32)


def mm_nt(a, b):
    return lax.dot_general(a, b, (((1,), (1,)), ((), ())), preferred_element_type=F32)


def mm_tn(a, b):
    return lax.dot_general(a, b, (((0,), (0,)), ((), ())), preferred_element_type=F32)


def iota(shape, dim):
    return lax.broadcasted_iota(jnp.int32, shape, dim)


def scaled_rows(wide, gain):
    return wide * lax.rsqrt(jnp.mean(wide * wide, axis=-1, keepdims=True) + EPS) * gain


def kernel(
    size, paired,
    x_ref, gain1_ref, wq_ref, wk_ref, wv_ref, first_ref, second_ref, bias_ref, extra_ref,
    hgain_ref, wo_ref, gain2_ref, wg_ref, wu_ref, wd_ref,
    out_ref,
    g_qkv, g_out, g_gu, g_dn,
    normed, decs, ends, qs, ks, vs, inside, ups_f, ups_b, car, headed, wout,
    place, hid, wide_gu, part_own, part_send, part_recv, ring_tx, ring_rx, own_res, full2, full3,
    z_send, z_recv, y_send, y_recv, rs_send, rs_recv, ag_send, ag_recv, out_sem,
):
    n, tp = size["fs"], size["tp"]
    chips = tp // 2
    far = chips // 2
    grp, me, t = lax.axis_index("grp"), lax.axis_index("fs"), lax.axis_index("tp")
    chip, core = t // 2, t % 2
    half = grp % 2 if paired else 0
    up_z, down_z = lax.rem(me + 1, n), lax.rem(me + n - 1, n)
    twin = grp + 1 - 2 * (grp % 2)
    mate = t + 1 - 2 * core
    right, left = lax.rem(t + 2, tp), lax.rem(t + tp - 2, tp)
    rows = x_ref.shape[0]
    share = rows // tp
    blocks = rows // BLOCK
    keyw = wq_ref.shape[1]
    valw = wv_ref.shape[1]
    wide = x_ref.shape[1]
    cols = wide // CHUNKS
    ffw = wg_ref.shape[1]
    whole = ffw // LANES * LANES
    rest = ffw - whole

    g_qkv[me, :, 0:keyw] = wq_ref[...]
    g_qkv[me, :, keyw : 2 * keyw] = wk_ref[...]
    g_qkv[me, :, 2 * keyw :] = wv_ref[...]
    g_out[me] = wo_ref[...]
    g_gu[me, :, 0:whole] = wg_ref[:, 0:whole]
    g_gu[me, :, whole : 2 * whole] = wu_ref[:, 0:whole]
    g_gu[me, :, 2 * whole :] = jnp.concatenate([wg_ref[:, whole:], wu_ref[:, whole:]], axis=1)
    dn_rows = wd_ref.shape[0]
    for c in range(CHUNKS):
        g_dn[c, me] = jnp.zeros(g_dn.shape[2:], BF16)
        g_dn[c, me, 0:dn_rows, :] = wd_ref[:, c * cols : (c + 1) * cols]

    barrier = pltpu.get_barrier_semaphore()
    friends = [{"fs": up_z}, {"fs": down_z}, {"tp": mate}, {"tp": right}, {"tp": left}]
    if paired:
        friends.append({"grp": twin})
    for friend in friends:
        pl.semaphore_signal(barrier, inc=1, device_id=friend, device_id_type=MESH)
    pl.semaphore_wait(barrier, len(friends))

    depth = wq_ref.shape[0]
    strip = depth // 2 if paired else depth
    gu_strip = strip // 2

    def part_of(ref, count, offset):
        base = half * (depth // 2) + offset
        return lambda slot: ref.at[slot, pl.ds(pl.multiple_of(base, 16), count), :]

    QKV, OUT, GUA, GUB, DNL, DNR = range(6)
    views = [
        part_of(g_qkv, strip, 0),
        lambda slot: g_out.at[slot],
        part_of(g_gu, gu_strip, 0),
        part_of(g_gu, gu_strip, gu_strip),
        lambda slot: g_dn.at[0, slot],
        lambda slot: g_dn.at[1, slot],
    ]
    crossing = {QKV: 0, GUA: 1, GUB: 2} if paired else {}
    hops = (n // 2, n - 1 - n // 2)

    def z_copy(p, way, s):
        slot = lax.rem(me - s + n, n) if way == 0 else lax.rem(me + s, n)
        view = views[p](slot)
        return pltpu.make_async_remote_copy(
            src_ref=view, dst_ref=view,
            send_sem=z_send.at[p, way, s], recv_sem=z_recv.at[p, way, s],
            device_id={"fs": up_z if way == 0 else down_z}, device_id_type=MESH,
        )

    def y_copy(p, way, s):
        slot = lax.rem(me - s - 1 + n, n) if way == 0 else lax.rem(me + s + 1, n)
        view = views[p](slot)
        return pltpu.make_async_remote_copy(
            src_ref=view, dst_ref=view,
            send_sem=y_send.at[crossing[p], way, s], recv_sem=y_recv.at[crossing[p], way, s],
            device_id={"grp": twin}, device_id_type=MESH,
        )

    def step(p, s, ways=(0, 1), arrive=True, leave=True):
        for way in ways:
            if arrive:
                z_copy(p, way, s - 1).wait_recv()
            if leave:
                z_copy(p, way, s).start()
            if arrive and p in crossing:
                y_copy(p, way, s - 1).start()

    def at(p, s):
        for way in (0, 1):
            if s <= hops[way]:
                step(p, s, (way,), arrive=s > 0, leave=s < hops[way])

    def y_arrived(p):
        if p in crossing:
            for way in (0, 1):

                @pl.loop(0, hops[way])
                def _(s):
                    y_copy(p, way, s).wait_recv()

    late = n // 4
    starts = {QKV: 0, OUT: 0, GUA: 0, GUB: late, DNL: n // 2, DNR: n // 2 + 2}
    queue = []

    def fill(lo, hi):
        for tick in range(lo, hi):
            queue.append([(p, tick - b) for p, b in starts.items() if 0 <= tick - b <= n // 2])

    def pump(count=1):
        for _ in range(count):
            if queue:
                for p, s in queue.pop(0):
                    at(p, s)

    low = iota((BLOCK, BLOCK), 0) >= iota((BLOCK, BLOCK), 1)
    high = iota((BLOCK, BLOCK), 0) <= iota((BLOCK, BLOCK), 1)

    def prepare(b):
        span = pl.ds(pl.multiple_of(b * BLOCK, BLOCK), BLOCK)
        tidy = scaled_rows(x_ref[span, :].astype(F32), gain1_ref[...]).astype(BF16)
        normed[span, :] = tidy
        lowrank = mm(tidy, first_ref[...]).astype(BF16)
        logits = mm(lowrank, second_ref[...]) + bias_ref[...]
        logsig = jnp.minimum(logits, 0.0) - jnp.log1p(jnp.exp(-jnp.abs(logits)))
        dec = logsig / GATE + extra_ref[span, :]
        one = dec.astype(BF16)
        left_over = dec - one.astype(F32)
        two = left_over.astype(BF16)
        three = (left_over - two.astype(F32)).astype(BF16)
        terms = jnp.concatenate([one, two, three], axis=1)
        for way, mask in ((0, low), (1, high)):
            sums = mm(jnp.where(mask, 1.0, 0.0).astype(BF16), terms)
            run = sums[:, 0:keyw] + sums[:, keyw : 2 * keyw] + sums[:, 2 * keyw :]
            mid_row = BLOCK // 2 - 1 if way == 0 else BLOCK // 2
            end_row = BLOCK - 1 if way == 0 else 0
            middle = run[mid_row : mid_row + 1, :]
            closing = run[end_row : end_row + 1, :]
            decs[way, 0, span, :] = jnp.exp(run)
            decs[way, 1, span, :] = jnp.exp(run - middle)
            decs[way, 2, span, :] = jnp.exp(middle - run)
            decs[way, 3, span, :] = jnp.exp(closing - run)
            ends[way, b] = jnp.broadcast_to(jnp.exp(closing), (8, keyw))

    for p in (QKV, OUT, GUA):
        at(p, 0)

    def early(lo, hi, pieces, with_rows):
        def body(tick, carry):
            for p in pieces:
                step(p, tick - starts[p])
            if with_rows:
                prepare(tick - 1)
            return carry

        lax.fori_loop(lo, hi, body, 0)

    ready = min(late - 1, blocks)
    if late > 1:
        early(1, 1 + ready, (QKV, OUT, GUA), True)
        if 1 + ready < late:
            early(1 + ready, late, (QKV, OUT, GUA), False)

    def rest_rows(b, carry):
        prepare(b)
        return carry

    at(QKV, late), at(OUT, late), at(GUA, late), at(GUB, 0)
    lax.fori_loop(ready, blocks, rest_rows, 0)
    last = max(n // 2 - 1, late + 1)
    if late + 1 < last:
        early(late + 1, last, (QKV, OUT, GUA, GUB), False)
    place_rows = iota(place.shape, 0)
    place_cols = iota(place.shape, 1)
    padded = g_dn.shape[2]
    place[...] = jnp.where(
        (place_rows // dn_rows == place_cols // padded)
        & (place_rows % dn_rows == place_cols % padded),
        1.0,
        0.0,
    ).astype(BF16)
    fill(last, n + 3)
    pump(2)
    y_arrived(QKV)

    def project(lo, hi):
        return mm(normed[...], g_qkv[:, :, lo:hi].reshape(n * depth, hi - lo)).astype(BF16)

    both = project(0, 2 * keyw)
    qs[...] = both[:, 0:keyw]
    ks[...] = both[:, keyw:]
    pump()
    vs[...] = project(2 * keyw, 2 * keyw + valw)
    pump()

    for b in range(blocks):
        span = slice(b * BLOCK, (b + 1) * BLOCK)
        q, k, v = qs[span, :].astype(F32), ks[span, :].astype(F32), vs[span, :]
        scores = 0.0
        for way, mask in ((0, low), (1, high)):
            pair = mm_nt(
                (q * decs[way, 1, span, :]).astype(BF16), (k * decs[way, 2, span, :]).astype(BF16)
            )
            scores = scores + jnp.where(mask, pair, 0.0)
            (ups_f, ups_b)[way][b] = mm_tn(v, (k * decs[way, 3, span, :]).astype(BF16))
        inside[span, :] = mm(scores.astype(BF16), v)
        if b % 2 == 1:
            pump()
    for way, ups, order in ((0, ups_f, range(blocks)), (1, ups_b, range(blocks - 1, -1, -1))):
        state = jnp.zeros((valw, keyw), F32)
        for b in order:
            car[b, :, way * keyw : (way + 1) * keyw] = state.astype(BF16)
            state = state * ends[way, b, 0:1, :] + ups[b]
    pump()
    wout[...] = g_out[...].astype(F32).reshape(wout.shape).astype(BF16)
    for b in range(blocks):
        span = slice(b * BLOCK, (b + 1) * BLOCK)
        q = qs[span, :].astype(F32)
        reach = jnp.concatenate(
            [(q * decs[0, 0, span, :]).astype(BF16), (q * decs[1, 0, span, :]).astype(BF16)], axis=1
        )
        mixed = inside[span, :] + mm_nt(reach, car[b])
        headed[b] = scaled_rows(mixed, hgain_ref[...]).astype(BF16)
        if b % 4 == 3:
            pump()

    low_rows, high_rows = slice(0, share // 2), slice(share // 2, share)

    def chip_rows(ref, which):
        return jnp.concatenate([ref[2 * i + which] for i in range(chips)], axis=0)

    def rs_copy(q, k, src, dst, to):
        return pltpu.make_async_remote_copy(
            src_ref=src, dst_ref=dst, send_sem=rs_send.at[q, k], recv_sem=rs_recv.at[q, k],
            device_id={"tp": to}, device_id_type=MESH,
        )

    def ring_copy(q, k):
        return rs_copy(q, 1 + k, ring_tx.at[q, k], ring_rx.at[q, k], right if k < 3 else left)

    def pair_copy(q):
        return rs_copy(q, 0, part_send.at[q], part_recv.at[q], mate)

    def rs_multiply(q, source, weight):
        other = mm(chip_rows(source, 1 - core), weight)
        part_send[q] = other.astype(BF16).reshape(part_send.shape[1:])
        pair_copy(q).start()
        part_own[q] = mm(chip_rows(source, core), weight).reshape(part_own.shape[1:])

    ahead, behind = lax.rem(chip + 1, chips), lax.rem(chip + chips - 1, chips)
    across = lax.rem(chip + far, chips)

    def chip_sum(q, which, span):
        return part_own[q, which, span, :] + part_recv[q, which, span, :].astype(F32)

    def rs_send_off(q):
        pair_copy(q).wait_recv()
        ring_tx[q, 0] = chip_sum(q, across, low_rows).astype(BF16)
        ring_tx[q, 3] = chip_sum(q, across, high_rows).astype(BF16)
        ring_copy(q, 0).start()
        ring_copy(q, 3).start()
        ring_tx[q, 1] = chip_sum(q, ahead, high_rows).astype(BF16)
        ring_tx[q, 4] = chip_sum(q, behind, low_rows).astype(BF16)
        ring_copy(q, 1).start()
        ring_copy(q, 4).start()

    def rs_relay(q):
        ring_copy(q, 0).wait_recv()
        ring_tx[q, 2] = (chip_sum(q, ahead, low_rows) + ring_rx[q, 0].astype(F32)).astype(BF16)
        ring_copy(q, 2).start()
        ring_copy(q, 3).wait_recv()
        ring_tx[q, 5] = (chip_sum(q, behind, high_rows) + ring_rx[q, 3].astype(F32)).astype(BF16)
        ring_copy(q, 5).start()

    def rs_finish(q):
        for k in (1, 2, 4, 5):
            ring_copy(q, k).wait_recv()
        top = chip_sum(q, chip, low_rows) + ring_rx[q, 2].astype(F32) + ring_rx[q, 4].astype(F32)
        end = chip_sum(q, chip, high_rows) + ring_rx[q, 1].astype(F32) + ring_rx[q, 5].astype(F32)
        return jnp.concatenate([top, end], axis=0)

    def ag_copy(a, k, buf):
        opposite = lax.rem(t + 2 * far, tp)
        slot, span, to = [
            (t, None, mate),
            (t, None, right),
            (t, None, left),
            (left, low_rows, right),
            (right, high_rows, left),
            (left, None, mate),
            (right, None, mate),
            (opposite, low_rows, mate),
            (opposite, high_rows, mate),
        ][k]
        view = buf.at[slot] if span is None else buf.at[slot, span, :]
        return pltpu.make_async_remote_copy(
            src_ref=view, dst_ref=view, send_sem=ag_send.at[a, k], recv_sem=ag_recv.at[a, k],
            device_id={"tp": to}, device_id_type=MESH,
        )

    def ag_start(a, buf):
        for k in (1, 2, 0):
            ag_copy(a, k, buf).start()

    def ag_relay(a, buf):
        ag_copy(a, 1, buf).wait_recv()
        ag_copy(a, 3, buf).start()
        ag_copy(a, 5, buf).start()
        ag_copy(a, 2, buf).wait_recv()
        ag_copy(a, 4, buf).start()
        ag_copy(a, 6, buf).start()

    def ag_finish(a, buf):
        ag_copy(a, 3, buf).wait_recv()
        ag_copy(a, 7, buf).start()
        ag_copy(a, 4, buf).wait_recv()
        ag_copy(a, 8, buf).start()
        for k in (0, 5, 6, 7, 8):
            ag_copy(a, k, buf).wait_recv()

    for c in range(CHUNKS):
        rs_multiply(c, headed, wout[:, c * cols : (c + 1) * cols])
        pump()
    for c in range(CHUNKS):
        rs_send_off(c)
        pump()
    for c in range(CHUNKS):
        rs_relay(c)
        pump()
    own_rows = pl.ds(pl.multiple_of(t * share, share), share)
    for c in range(CHUNKS):
        span = slice(c * cols, (c + 1) * cols)
        own_res[:, span] = (x_ref[own_rows, span].astype(F32) + rs_finish(c)).astype(BF16)
    full2[t] = scaled_rows(own_res[...].astype(F32), gain2_ref[...]).astype(BF16)
    ag_start(0, full2)
    pump(2)
    ag_relay(0, full2)
    pump(2)
    ag_finish(0, full2)
    while sum(len(q) for q in queue if any(p == GUB for p, _ in q)):
        pump()
    y_arrived(GUA)
    y_arrived(GUB)

    normed2 = full2[...].reshape(rows, wide)
    for lo in range(0, 2 * ffw, 2 * LANES):
        hi = min(lo + 2 * LANES, 2 * ffw)
        wide_gu[:, lo:hi] = mm(normed2, g_gu[:, :, lo:hi].reshape(n * depth, hi - lo))
    for i in range(tp):
        span = slice(i * share, (i + 1) * share)
        tail = wide_gu[span, 2 * whole :]
        gate = jnp.concatenate([wide_gu[span, 0:whole], tail[:, 0:rest]], axis=1)
        up = jnp.concatenate([wide_gu[span, whole : 2 * whole], tail[:, rest:]], axis=1)
        hidden = (gate / (1.0 + jnp.exp(-gate)) * up).astype(BF16)
        hid[i] = mm(hidden, place[...]).astype(BF16)
    pump()

    for c in range(CHUNKS):
        while sum(len(q) for q in queue if any(p == DNL + c for p, _ in q)):
            pump()
        q = CHUNKS + c
        weight = g_dn[c].astype(F32).reshape(n * padded, cols).astype(BF16)
        rs_multiply(q, hid, weight)
        if c > 0:
            rs_relay(q - 1)
        rs_send_off(q)

    def finish(c):
        span = slice(c * cols, (c + 1) * cols)
        done = own_res[:, span].astype(F32) + rs_finish(CHUNKS + c)
        full3[c, t] = done.astype(BF16)
        ag_start(1 + c, full3.at[c])

    def put(c):
        return pltpu.make_async_copy(
            full3.at[c], out_ref.at[:, :, c * cols : (c + 1) * cols], out_sem.at[c]
        )

    finish(0)
    rs_relay(CHUNKS + 1)
    ag_relay(1, full3.at[0])
    finish(1)
    ag_finish(1, full3.at[0])
    put(0).start()
    ag_relay(2, full3.at[1])
    ag_finish(2, full3.at[1])
    put(1).start()

    for p in range(len(views)):
        for way in (0, 1):

            @pl.loop(0, hops[way])
            def _(s):
                z_copy(p, way, s).wait_send()
                if p in crossing:
                    y_copy(p, way, s).wait_send()

    for q in range(2 * CHUNKS):
        pair_copy(q).wait_send()
        for k in range(6):
            ring_copy(q, k).wait_send()
    for a, buf in ((0, full2), (1, full3.at[0]), (2, full3.at[1])):
        for k in range(9):
            ag_copy(a, k, buf).wait_send()
    for c in range(CHUNKS):
        put(c).wait()


def shards(size, *args):
    (x, gain1, wq, wk, wv, first, second, bias, extra, hgain, wo, gain2, wg, wu, wd) = args
    n, tp = size["fs"], size["tp"]
    paired = size["grp"] % 2 == 0
    rows, wide = x.shape
    depth, keyw = wq.shape
    valw, ffw = wv.shape[1], wg.shape[1]
    share, chips, blocks = rows // tp, tp // 2, rows // BLOCK
    cols = wide // CHUNKS
    padded = -(-wd.shape[0] // 8) * 8
    sems = pltpu.SemaphoreType.DMA
    vmem = pltpu.VMEM
    steps = n // 2
    out = pl.pallas_call(
        functools.partial(kernel, size, paired),
        out_shape=jax.ShapeDtypeStruct((tp, share, wide), BF16),
        in_specs=[pl.BlockSpec(memory_space=pltpu.VMEM)] * 15,
        out_specs=pl.BlockSpec(memory_space=pl.ANY),
        scratch_shapes=[
            vmem((n, depth, 2 * keyw + valw), BF16),
            vmem((n, wo.shape[0], wide), BF16),
            vmem((n, depth, 2 * ffw), BF16),
            vmem((CHUNKS, n, padded, cols), BF16),
            vmem((rows, wide), BF16),
            vmem((2, 4, rows, keyw), F32),
            vmem((2, blocks, 8, keyw), F32),
            vmem((rows, keyw), BF16),
            vmem((rows, keyw), BF16),
            vmem((rows, valw), BF16),
            vmem((rows, valw), F32),
            vmem((blocks, valw, keyw), F32),
            vmem((blocks, valw, keyw), F32),
            vmem((blocks, valw, 2 * keyw), BF16),
            vmem((blocks, BLOCK, valw), BF16),
            vmem((n * wo.shape[0], wide), BF16),
            vmem((ffw, n * padded), BF16),
            vmem((tp, share, n * padded), BF16),
            vmem((rows, 2 * ffw), F32),
            vmem((2 * CHUNKS, chips, share, cols), F32),
            vmem((2 * CHUNKS, chips, share, cols), BF16),
            vmem((2 * CHUNKS, chips, share, cols), BF16),
            vmem((2 * CHUNKS, 6, share // 2, cols), BF16),
            vmem((2 * CHUNKS, 6, share // 2, cols), BF16),
            vmem((share, wide), BF16),
            vmem((tp, share, wide), BF16),
            vmem((CHUNKS, tp, share, cols), BF16),
            sems((6, 2, steps)),
            sems((6, 2, steps)),
            sems((3, 2, steps)),
            sems((3, 2, steps)),
            sems((2 * CHUNKS, 7)),
            sems((2 * CHUNKS, 7)),
            sems((1 + CHUNKS, 9)),
            sems((1 + CHUNKS, 9)),
            sems((CHUNKS,)),
        ],
        compiler_params=pltpu.CompilerParams(
            collective_id=0, has_side_effects=True, vmem_limit_bytes=64 * 1024 * 1000
        ),
        name="layer",
    )(
        x, gain1.reshape(1, -1), wq, wk, wv, first, second, bias.reshape(1, -1), extra,
        hgain.reshape(1, -1), wo, gain2.reshape(1, -1), wg, wu, wd,
    )
    return out.reshape(rows, wide)


def solution(mesh):
    placed = (
        P(("grp", "fs"), None),
        P(),
        P("fs", "tp"),
        P("fs", "tp"),
        P("fs", "tp"),
        P(),
        P(None, "tp"),
        P("tp"),
        P(("grp", "fs"), "tp"),
        P(),
        P(("tp", "fs"), None),
        P(),
        P("fs", "tp"),
        P("fs", "tp"),
        P(("tp", "fs"), None),
    )
    return jax.shard_map(
        functools.partial(shards, dict(mesh.shape)),
        mesh=mesh, in_specs=placed, out_specs=P(("grp", "fs"), None), check_vma=False,
    )
```

time: 583 us -> 230 us (0.39)
  waiting for transfers between devices: 301 us -> 0 us
  Pallas kernels: 0 us -> 223 us
  blocking collectives: 81.3 us -> 0 us
  matrix products: 74.3 us -> 0 us
  starting transfers between devices: 68.7 us -> 0 us
  local copies, waits for them, and re-layouts: 29.1 us -> 6.56 us
  between operations: 13.4 us -> 0.01 us
  other arithmetic: 9.12 us -> 0 us
    all_gather x3 -> x0, waiting for transfers between devices: 274 us -> none  [the longest x2 274 us: sent_together(): whole = lax.all_gather(both, axis, axis=dim, tiled=True)]
    pallas_call x0 -> x1, Pallas kernels: none -> 223 us  [shards(): pl.pallas_call(functools.partial(kernel, size, paired), out_shape=jax.Sha...]
    all_to_all x2 -> x0, blocking collectives: 81.3 us -> none  [the longest x1 51.5 us: sent_and_summed(): lax.all_to_all(tiles, axis, split_axis=0, concat_axis=0, tiled=True)]
    dot_general x55 -> x0, matrix products: 74.3 us -> none  [the longest x16 17.1 us: advance(): inside = jnp.dot(scores, value_block)]
    all_to_all x3 -> x0, starting transfers between devices: 68.5 us -> none  [the longest x2 50.9 us: sent_to_all(): return lax.all_to_all(copies, axis, split_axis=0, concat_axis=0, tiled=True)]
    all_to_all x3 -> x0, waiting for transfers between devices: 26.3 us -> none  [the longest x1 26.3 us: sent_and_summed(): lax.all_to_all(tiles, axis, split_axis=0, concat_axis=0, tiled=True)]
    squeeze x16 -> x0, local copies, waits for them, and re-layouts: 12.3 us -> none  [block_scan(): lax.scan(advance, jnp.zeros((key_channel_width, value_width), jnp.float32...]
    another operation x6 -> x0, local copies, waits for them, and re-layouts: 6.8 us -> none
  transfers between devices with their start and end apart: 6 -> 0, of which waited for: 3 -> 0; matrix products, arithmetic and copies ran while one was open for 16% -> 0% of each run, Pallas kernels for 0% -> 0%
where the time goes in v1:
time: 230 us; the launch traced here: 229 us
  Pallas kernels  223 us (97%)
  local copies, waits for them, and re-layouts  6.56 us (3%)
    pallas_call x1, Pallas kernels, shards(): pl.pallas_call(functools.partial(kernel, size, paired), out_shape=jax.Sha...  223 us
    unnamed x3, local copies, waits for them, and re-layouts  6.56 us

profile of v1, /device:TPU:33, one launch (start us, length us, event | category | flops | bytes accessed | tf_op | source)
XLA Modules:
  0.0 229.4 jit_solution(9703192047106305791)
XLA Ops:
  0.0 1.6 copy.17.extra_ref
  1.6 1.8 copy.16.first_ref
  3.4 222.8 %layer.1 = bf16[8,64,2048]{2,1,0:T(8,128)(2,1)} custom-call(bf16[512,2048]{1,0:T(8,128)(2,1)} %x_ref.1, f32[1,2048]{1,0:T(1,128)} %bitcast.6, bf16[64,128]{1,0:T(8,128)(2,1)} %wq_ref.1, bf16[64,128]{1,0:T(8,128)(2,1)} %wk_ref.1, bf16[64,256]{1,0:T(8,128)(2,1)} %wv_ref.1, bf16[2048,16]{1,0:T(8,128)(2,1)} %copy.16.first_ref, bf16[16,128]{1,0:T(8,128)(2,1)} %second_ref.1, ...), custom_call_target="tpu_custom_call" | custom-call | tf_op jit(solution)/shard_map/layer/pallas_call | solution.py:471
  226.3 3.2 %copy.19 = bf16[512,2048]{1,0:T(8,128)(2,1)} copy(bf16[512,2048]{1,0:T(8,128)(2,1)} %bitcast.5) | data formatting | bytes 4194304
